TPU v7x, 32 devices: a whole 2x2x4 slice. The times are simulated.
32 devices in a mesh: sp: 4 (over z), fs: 4 (over y, x), tp: 2 (over core).
Axes of the slice: x: 2, y: 2, z: 4, core: 2. Of those that a mesh axis runs over, the one named last changes fastest.
Arguments:
- tokens: bfloat16 [4, 3072, 2048], P('fs', 'sp'), may hold values from -6 to 6
- norm_gain: float32 [2048], replicated, may hold values from 0.1 to 1.9
- w_query: bfloat16 [2048, 512], P('sp', 'tp'), may hold values from -0.125 to 0.125
- w_key: bfloat16 [2048, 512], P('sp', 'tp'), may hold values from -0.125 to 0.125
- w_value: bfloat16 [2048, 1024], P('sp', 'tp'), may hold values from -0.125 to 0.125
- w_conv_value: bfloat16 [2048, 1024], P('sp', 'tp'), may hold values from -0.125 to 0.125
- w_conv_gate: bfloat16 [2048, 1024], P('sp', 'tp'), may hold values from -0.125 to 0.125
- w_decay_low: bfloat16 [2048, 16], replicated, may hold values from -0.125 to 0.125
- w_decay_high: bfloat16 [16, 512], replicated, may hold values from -1.5 to 1.5
- gate_bias: float32 [512], replicated, may hold values from 0.5 to 10
- decay_shift: float32 [4, 3072, 512], P('fs', 'sp', 'tp'), may hold values from -0.6 to 0
- head_gain: float32 [512], replicated, may hold values from 0.1 to 1.9
- conv_taps: float32 [31, 1024], replicated, may hold values from -15 to 15
- channel_gain: float32 [1024], replicated, may hold values from 0.1 to 1.9
- w_out_attn: bfloat16 [1024, 2048], P('tp', 'sp'), may hold values from -0.125 to 0.125
- w_out_conv: bfloat16 [1024, 2048], P('tp', 'sp'), may hold values from -0.125 to 0.125
- init_state: float32 [4, 2, 256, 512], P('fs', 'tp'), may hold values from -332.55374 to 332.55374
Outputs:
- mixed: bfloat16 [4, 3072, 2048], P('fs', ('sp', 'tp'))
All inputs are finite; a program needn't handle non-finite values.
Results may differ from a plain program's by a relative error of at most 0.0056.
The roundings to bfloat16 on the way count: a program that leaves them out, or rounds other values in their place, can miss the bound.
Values may be sent and summed in bfloat16 or wider, within the bound.
A program may use at most 128 MiB of HBM per device.

v0:
```python
import jax
import jax.numpy as jnp
from jax import lax
from jax.sharding import PartitionSpec as P

DK = 256
DV = 512
CW = 1024
KW = 31
BLOCK = 64


RMS_EPS = 1e-06
LN_EPS = 1e-05
GATE_NORMALIZER = 16.0
UPPER_PRECISION = lax.Precision.HIGHEST


def entering(array, axis, combine, identity):
    size, place = (lax.axis_size(axis), lax.axis_index(axis))
    everything = jax.tree.map(lambda part: lax.all_gather(part, axis), array)
    start = jax.tree.map(
        lambda part, zero: jnp.broadcast_to(jnp.asarray(zero, part.dtype), part.shape),
        array,
        identity,
    )

    def turn(k, before):
        reached = k < place
        new = combine(before, jax.tree.map(lambda part: part[k], everything))
        return jax.tree.map(lambda a, b: jnp.where(reached, a, b), new, before)

    return lax.fori_loop(0, size, turn, start)


def shifted(value, axis, steps):
    count = lax.axis_size(axis)
    initial, last = (max(0, -steps), min(count, count - steps))
    return lax.ppermute(value, axis, [(source, source + steps) for source in range(initial, last)])


def rounded(array):
    return lax.optimization_barrier(array.astype(jnp.bfloat16)).astype(jnp.float32)


def chain_combine(earlier, later):
    return (earlier[0] * later[0], later[0][..., None] * earlier[1] + later[1])


def on_device(
    tokens,
    norm_gain,
    w_query,
    w_key,
    w_value,
    w_conv_value,
    w_conv_gate,
    w_decay_low,
    w_decay_high,
    gate_bias,
    decay_shift,
    head_gain,
    conv_taps,
    channel_gain,
    w_out_attn,
    w_out_conv,
    init_state,
):
    token_rows = tokens[0].astype(jnp.float32)
    length_here = token_rows.shape[0]
    normed = (
        token_rows
        * lax.rsqrt(jnp.mean(token_rows * token_rows, axis=1, keepdims=True) + RMS_EPS)
        * norm_gain
    ).astype(jnp.bfloat16)
    position = lax.axis_index("tp")
    key_cols = w_query.shape[1]
    value_cols = w_value.shape[1]
    conv_cols = w_conv_value.shape[1]
    heads_here = key_cols // DK
    pieces = (
        lax.all_gather(w_query, "sp", axis=0, tiled=True),
        lax.all_gather(w_key, "sp", axis=0, tiled=True),
        lax.all_gather(w_value, "sp", axis=0, tiled=True),
        lax.all_gather(w_conv_value, "sp", axis=0, tiled=True),
        lax.all_gather(w_conv_gate, "sp", axis=0, tiled=True),
    )
    queries, keys_proj, values_proj, conv_value, conv_gate = tuple(
        (
            jnp.dot(normed, weight_piece, preferred_element_type=jnp.float32)
            for weight_piece in pieces
        )
    )
    low_rank = jnp.dot(normed, w_decay_low, preferred_element_type=jnp.float32).astype(jnp.bfloat16)
    high_cols = lax.dynamic_slice_in_dim(w_decay_high, position * key_cols, key_cols, 1)
    bias_here = lax.dynamic_slice_in_dim(gate_bias, position * key_cols, key_cols, 0)
    log_decay = (
        jax.nn.log_sigmoid(
            jnp.dot(low_rank, high_cols, preferred_element_type=jnp.float32) + bias_here
        )
        / GATE_NORMALIZER
        + decay_shift[0]
    )
    nblocks = length_here // BLOCK

    def blocks_of(array, width):
        return array.reshape(nblocks, BLOCK, heads_here, width).transpose(2, 0, 1, 3)

    query_blocks = blocks_of(rounded(queries), DK) * DK ** (-0.5)
    key_blocks = blocks_of(rounded(keys_proj), DK)
    value_blocks = blocks_of(rounded(values_proj), DV)
    decay_blocks = blocks_of(log_decay, DK)
    running_total = jnp.cumsum(decay_blocks, axis=2)
    final_entry = running_total[:, :, -1:, :]
    scaled_query = query_blocks * jnp.exp(running_total)
    key_scaled = key_blocks * jnp.exp(-running_total)
    lower = jnp.tril(jnp.ones((BLOCK, BLOCK), jnp.float32))
    attention_scores = (
        jnp.einsum("hnik,hnjk->hnij", scaled_query, key_scaled, precision=UPPER_PRECISION) * lower
    )
    inner = jnp.einsum("hnij,hnjv->hniv", attention_scores, value_blocks, precision=UPPER_PRECISION)
    updates = jnp.einsum(
        "hnjk,hnjv->hnkv",
        key_blocks * jnp.exp(final_entry - running_total),
        value_blocks,
        precision=UPPER_PRECISION,
    )
    block_decay = jnp.exp(final_entry[:, :, 0, :])

    def carry_step(recurrent_state, items):
        decay_now, update_now = items
        return (decay_now[..., None] * recurrent_state + update_now, recurrent_state)

    local_end, before = lax.scan(
        carry_step,
        jnp.zeros((heads_here, DK, DV), jnp.float32),
        (block_decay.transpose(1, 0, 2), updates.transpose(1, 0, 2, 3)),
    )
    inner = inner + jnp.einsum("hnik,nhkv->hniv", scaled_query, before, precision=UPPER_PRECISION)
    start_positions = jnp.cumsum(final_entry, axis=1) - final_entry
    device_decay = jnp.exp(jnp.sum(final_entry[:, :, 0, :], axis=1))
    decay_before, state_before = entering(
        (device_decay, local_end),
        "sp",
        chain_combine,
        (jnp.ones_like(device_decay), jnp.zeros_like(local_end)),
    )
    incoming_carry = state_before + decay_before[..., None] * init_state[0]
    attended = inner + jnp.einsum(
        "stcl,slu->stcu",
        scaled_query * jnp.exp(start_positions),
        incoming_carry,
        precision=UPPER_PRECISION,
    )
    mean_square = jnp.mean(attended * attended, axis=3, keepdims=True)
    attn_out = (attended * lax.rsqrt(mean_square + RMS_EPS) * head_gain).astype(jnp.bfloat16)
    attn_out = attn_out.transpose(1, 2, 0, 3).reshape(length_here, value_cols)
    glu = (conv_value * jax.nn.sigmoid(conv_gate)).astype(jnp.bfloat16)
    rim = shifted(glu[length_here - (KW - 1) :], "sp", 1)
    padded = jnp.concatenate([rim, glu], axis=0).astype(jnp.float32)
    taps_here = lax.dynamic_slice_in_dim(conv_taps, position * conv_cols, conv_cols, 1)
    filtered = jnp.zeros((length_here, conv_cols), jnp.float32)
    for tap_index in range(KW):
        filtered = filtered + taps_here[tap_index] * padded[tap_index : tap_index + length_here]
    first_sum, square_sum = lax.psum(
        (
            jnp.sum(filtered, axis=1, keepdims=True),
            jnp.sum(filtered * filtered, axis=1, keepdims=True),
        ),
        "tp",
    )
    mean = first_sum / CW
    centered = filtered - mean
    variance = square_sum / CW - mean * mean
    gain_here = lax.dynamic_slice_in_dim(channel_gain, position * conv_cols, conv_cols, 0)
    conv_out = jax.nn.silu(centered * lax.rsqrt(variance + LN_EPS) * gain_here).astype(jnp.bfloat16)
    pieces = (
        lax.all_gather(w_out_attn, "sp", axis=1, tiled=True),
        lax.all_gather(w_out_conv, "sp", axis=1, tiled=True),
    )
    columns = jnp.dot(attn_out, pieces[0], preferred_element_type=jnp.float32) + jnp.dot(
        conv_out, pieces[1], preferred_element_type=jnp.float32
    )
    mixed = lax.psum_scatter(columns, "tp", scatter_dimension=0, tiled=True)
    return mixed.astype(jnp.bfloat16)[None]


def solution(mesh):
    in_specs = (
        P("fs", "sp", None),
        P(),
        P("sp", "tp"),
        P("sp", "tp"),
        P("sp", "tp"),
        P("sp", "tp"),
        P("sp", "tp"),
        P(),
        P(),
        P(),
        P("fs", "sp", "tp"),
        P(),
        P(),
        P(),
        P("tp", "sp"),
        P("tp", "sp"),
        P("fs", "tp", None, None),
    )
    out_specs = P("fs", ("sp", "tp"), None)
    return jax.shard_map(
        on_device, mesh=mesh, in_specs=in_specs, out_specs=out_specs, check_vma=False
    )
```

profile of v0, /device:TPU:1, one launch (start us, length us, event | category | flops | bytes accessed | tf_op | source)
XLA Modules:
  0.0 376.7 jit_solution(12193820177922108319)
XLA Ops:
  10.0 2.6 fusion.1
  12.6 4.4 %fusion.3 = bf16[768,2048]{1,0:T(8,128)(2,1)} fusion(bf16[1,768,2048]{2,1,0:T(8,128)(2,1)} %param.21, f32[2048]{0:T(1024)S(1)} %copy-done.9, f32[768]{0:T(1024)S(1)} %add_rsqrt_fusion.1), kind=kLoop, calls=%fused_computation.12 | loop fusion | flops 6291456 | bytes 6302720 | tf_op jit(solution)/shard_map/convert_element_type | solution.py:75
  17.1 3.5 fusion.41
  21.4 17.1 %all-gather.14.cloned.1.call-done = bf16[2048,256]{1,0:T(8,128)(2,1)} async-done(((bf16[512,256]{1,0:T(8,128)(2,1)}), bf16[2048,256]{1,0:T(8,128)(2,1)}) %all-gather.14.cloned.1.call-update) | async-done | bytes 1048592 | tf_op jit(solution)/shard_map/all_gather | solution.py:83
  38.5 3.1 convolution_convert_fusion.1
  41.7 43.8 %all-gather.16.cloned.1.call-done = bf16[2048,512]{1,0:T(8,128)(2,1)} async-done(((bf16[512,512]{1,0:T(8,128)(2,1)}), bf16[2048,512]{1,0:T(8,128)(2,1)}) %all-gather.16.cloned.1.call-update) | async-done | bytes 2097168 | tf_op jit(solution)/shard_map/all_gather | solution.py:84
  85.5 4.3 %convolution_convert_fusion = bf16[768,512]{1,0:T(8,128)(2,1)S(1)} fusion(bf16[768,2048]{1,0:T(8,128)(2,1)} %fusion.3, bf16[2048,512]{1,0:T(8,128)(2,1)} %all-gather.16.cloned.1.call-done), kind=kOutput, calls=%fused_computation.86 | convolution fusion | flops 1611005952 | bytes 6029312 | tf_op jit(solution)/shard_map/dot_general | solution.py:90
  89.8 4.7 %convolution_bitcast_fusion = f32[12,1,256,512]{3,2,1,0:T(8,128)} fusion(bf16[12,64,512]{2,1,0:T(8,128)(2,1)S(1)} %bitcast.149, bf16[12,64,256]{2,1,0:T(8,128)(2,1)S(1)} %bitcast.151, f32[1,12,64,256]{3,1,2,0:T(8,128)S(1)} %get-tuple-element.287, f32[12,256]{1,0:T(8,128)S(1)} %get-tuple-element.249), kind=kOutput, calls=%fused_computation.16 | convolution fusion | flops 1208549376 | bytes 8269824 | tf_op jit(solution)/shard_map/hnjk,hnjv->hnkv/dot_general | solution.py:122
  94.5 24.3 %while.32 = (s32[]{:T(128)}, f32[1,256,512]{2,1,0:T(8,128)S(1)}, f32[12,1,256,512]{3,2,1,0:T(8,128)}, f32[12,1,256]{2,0,1:T(8,128)S(1)}, f32[12,1,256,512]{3,2,1,0:T(8,128)}, /*index=5*/s32[]{:T(128)}, s32[]{:T(128)}) while((s32[]{:T(128)}, f32[1,256,512]{2,1,0:T(8,128)S(1)}, f32[12,1,256,512]{3,2,1,0:T(8,128)}, ...), condition=%wide.region_3.4_spmd.clone, body=%wide.region_2.3_spmd.clone.sunk | while | flops 524291 | bytes 2624620 | solution.py:134
  95.4 1.2 bitcast_add_fusion.3
  97.4 1.2 bitcast_add_fusion.3
  99.4 1.2 bitcast_add_fusion.3
  101.4 1.2 bitcast_add_fusion.3
  103.5 1.2 bitcast_add_fusion.3
  105.5 1.2 bitcast_add_fusion.3
  107.5 1.2 bitcast_add_fusion.3
  109.5 1.2 bitcast_add_fusion.3
  111.6 1.2 bitcast_add_fusion.3
  113.6 1.2 bitcast_add_fusion.3
  115.6 1.2 bitcast_add_fusion.3
  117.6 1.2 bitcast_add_fusion.3
  121.7 7.8 %all-gather.2 = f32[4,1,256]{2,1,0:T(1,128)S(1)} all-gather(f32[1,1,256]{2,1,0:T(1,128)S(1)} %bitcast.188), channel_id=2, replica_groups=mesh['sp'=4,'fs'=4,'tp'=2] {'sp'}, dimensions={0}, use_global_device_ids=true | all-gather | bytes 5120 | tf_op jit(solution)/shard_map/all_gather | solution.py:21
  129.6 1.2 fusion.67
  130.8 1.4 constant_dynamic-slice_fusion.2
  132.2 3.2 convolution_convert_fusion.2
  136.4 1.8 convolution_multiply_fusion
  138.2 22.2 %all-gather.20.cloned.1.call-done = bf16[2048,512]{1,0:T(8,128)(2,1)} async-done(((bf16[512,512]{1,0:T(8,128)(2,1)}), bf16[2048,512]{1,0:T(8,128)(2,1)}) %all-gather.20.cloned.1.call-update) | async-done | bytes 2097168 | tf_op jit(solution)/shard_map/all_gather | solution.py:85
  160.4 5.5 %fusion.70 = f32[768,512]{1,0:T(8,128)} fusion(bf16[768,2048]{1,0:T(8,128)(2,1)} %fusion.3, bf16[2048,512]{1,0:T(8,128)(2,1)} %all-gather.20.cloned.1.call-done), kind=kOutput, calls=%fused_computation.140 | convolution fusion | flops 1610612736 | bytes 6815744 | tf_op jit(solution)/shard_map/dot_general | solution.py:90
  165.9 40.4 %all-gather.22.cloned.1.call-done = bf16[2048,512]{1,0:T(8,128)(2,1)} async-done(((bf16[512,512]{1,0:T(8,128)(2,1)}), bf16[2048,512]{1,0:T(8,128)(2,1)}) %all-gather.22.cloned.1.call-update) | async-done | bytes 2097168 | tf_op jit(solution)/shard_map/all_gather | solution.py:86
  206.2 5.0 %multiply_convert_fusion.1 = bf16[768,512]{1,0:T(8,128)(2,1)S(1)} fusion(f32[768,512]{1,0:T(8,128)} %fusion.70, bf16[768,2048]{1,0:T(8,128)(2,1)} %fusion.3, bf16[2048,512]{1,0:T(8,128)(2,1)} %all-gather.22.cloned.1.call-done), kind=kOutput, calls=%fused_computation.82 | convolution fusion | flops 1612578816 | bytes 7602176 | tf_op jit(solution)/shard_map/dot_general | solution.py:90
  211.2 1.5 collective-permute-start
  212.7 8.5 %fusion.4 = f32[12,64,512]{2,1,0:T(8,128)} fusion(f32[12,1,256,512]{3,2,1,0:T(8,128)} %get-tuple-element.143, f32[12,64,256]{2,1,0:T(8,128)S(1)} %bitcast.145, f32[1,12,64,256]{3,1,2,0:T(8,128)S(1)} %get-tuple-element.287), kind=kOutput, calls=%fused_computation.13 | convolution fusion | flops 1208156160 | bytes 9437184 | tf_op jit(solution)/shard_map/hnik,nhkv->hniv/dot_general | solution.py:139
  221.5 6.8 %fusion.65 = (f32[768]{0:T(1024)S(1)}, f32[768]{0:T(1024)S(1)}, f32[768,512]{1,0:T(8,128)S(1)}) fusion(f32[798,512]{1,0:T(8,128)S(1)} %maximum_convert_fusion, f32[512]{0:T(512)S(1)} %bitcast.169, f32[512]{0:T(512)S(1)} %bitcast.171, f32[512]{0:T(512)S(1)} %bitcast.172, f32[512]{0:T(512)S(1)} %bitcast.173, f32[512]{0:T(512)S(1)} %bitcast.174, ...), kind=kLoop, calls=%fused_computation.136 | loop fusion | flops 25164288 | bytes 50401280 | tf_op jit(solution)/shard_map/reduce_sum | solution.py:167
  228.3 3.8 %all-reduce = (f32[768,1]{0,1:T(1,128)S(1)}, f32[768,1]{0,1:T(1,128)S(1)}) all-reduce(f32[768,1]{0,1:T(1,128)S(1)} %broadcast_in_dim.39, f32[768,1]{0,1:T(1,128)S(1)} %broadcast_in_dim.40), channel_id=1, replica_groups=mesh['sp'=4,'fs'=4,'tp'=2] {'tp'}, use_global_device_ids=true, to_apply=%region_10.11 | all-reduce | flops 1536 | bytes 12288 | tf_op jit(solution)/shard_map/psum | solution.py:165
  232.1 20.1 %all-gather.26.cloned.1.call-done = f32[4,256,512]{2,1,0:T(8,128)} async-done(((f32[1,256,512]{2,1,0:T(8,128)}), f32[4,256,512]{2,1,0:T(8,128)}) %all-gather.26.cloned.1.call-update) | async-done | bytes 2097168 | tf_op jit(solution)/shard_map/all_gather | solution.py:21
  252.2 4.9 %while.33 = (s32[]{:T(128)}, f32[1,256]{1,0:T(1,128)S(1)}, f32[1,256,512]{2,1,0:T(8,128)S(1)}, s32[]{:T(128)}, f32[4,1,256]{2,1,0:T(1,128)S(1)}, /*index=5*/f32[4,1,256,512]{3,2,1,0:T(8,128)}, s32[]{:T(128)}, s32[]{:T(128)}) while((s32[]{:T(128)}, f32[1,256]{1,0:T(1,128)S(1)}, f32[1,256,512]{2,1,0:T(8,128)S(1)}, s32[]{:T(128)}, ...), condition=%wide.region_7.8_spmd.clone, body=%wide.region_6.7_spmd.clone.sunk | while | flops 525060 | bytes 1578107 | solution.py:33
  252.2 1.2 fusion.91
  253.5 1.2 fusion.91
  254.7 1.2 fusion.91
  255.9 1.2 fusion.91
  257.1 2.7 fusion.51
  259.9 1.1 multiply_reduce_fusion.1
  261.2 37.0 %all-gather.18.cloned.1.call-done = bf16[512,2048]{1,0:T(8,128)(2,1)} async-done(((bf16[512,512]{1,0:T(8,128)(2,1)}), bf16[512,2048]{1,0:T(8,128)(2,1)}) %all-gather.18.cloned.1.call-update) | async-done | bytes 2097168 | tf_op jit(solution)/shard_map/all_gather | solution.py:178
  298.2 6.0 %fusion.69 = f32[768,2048]{1,0:T(8,128)} fusion(bf16[768,512]{1,0:T(8,128)(2,1)S(1)} %bitcast.147, bf16[512,2048]{1,0:T(8,128)(2,1)} %all-gather.18.cloned.1.call-done), kind=kOutput, calls=%fused_computation.139 | convolution fusion | flops 1610612736 | bytes 9175040 | tf_op jit(solution)/shard_map/dot_general | solution.py:181
  304.3 40.0 %all-gather.24.cloned.1.call-done = bf16[512,2048]{1,0:T(8,128)(2,1)} async-done(((bf16[512,512]{1,0:T(8,128)(2,1)}), bf16[512,2048]{1,0:T(8,128)(2,1)}) %all-gather.24.cloned.1.call-update) | async-done | bytes 2097168 | tf_op jit(solution)/shard_map/all_gather | solution.py:179
  344.3 8.1 %convolution_add_fusion = f32[768,2048]{1,0:T(8,128)} fusion(f32[768,2048]{1,0:T(8,128)} %fusion.69, bf16[512,2048]{1,0:T(8,128)(2,1)} %all-gather.24.cloned.1.call-done, f32[768,512]{1,0:T(8,128)S(1)} %get-tuple-element.248, f32[512]{0:T(512)S(1)} %dynamic_slice.37, f32[768]{0:T(1024)S(1)} %get-tuple-element.221, f32[768]{0:T(1024)S(1)} %get-tuple-element.220), kind=kOutput, calls=%fused_computation.15 | convolution fusion | flops 1615331328 | bytes 16261120 | tf_op jit(solution)/shard_map/dot_general | solution.py:181
  352.5 14.4 %reduce-scatter.2.cloned.1.call-done = f32[384,2048]{1,0:T(8,128)} async-done(((f32[768,2048]{1,0:T(8,128)}), f32[384,2048]{1,0:T(8,128)}) %reduce-scatter.2.cloned.1.call-update) | async-done | bytes 3145744 | tf_op jit(solution)/shard_map/reduce_scatter | solution.py:184
  366.9 3.3 convert_bitcast_fusion
  (100 shorter events, 18.9 us)
Async XLA Ops:
  6.5 10.6 %copy-start = (bf16[2048,16]{0,1:T(8,128)(2,1)S(1)}, bf16[2048,16]{0,1:T(8,128)(2,1)}, u32[]{:S(2)}) copy-start(bf16[2048,16]{0,1:T(8,128)(2,1)} %param.28) | copy-start | bytes 196612
  6.5 32.0 %all-gather.14.cloned.1.call-start = ((), (), s32[]{:S(2)}) async-start(), calls=%async_computation.2 | async-start | bytes 1310720 | tf_op jit(solution)/shard_map/all_gather | solution.py:83
  7.3 78.2 %all-gather.16.cloned.1.call-start = ((), (), s32[]{:S(2)}) async-start(), calls=%async_computation.3 | async-start | bytes 2621440 | tf_op jit(solution)/shard_map/all_gather | solution.py:84
  8.0 124.2 %all-gather.12.cloned.1.call-start = ((), (), s32[]{:S(2)}) async-start(), calls=%async_computation.1 | async-start | bytes 1310720 | tf_op jit(solution)/shard_map/all_gather | solution.py:82
  8.7 151.7 %all-gather.20.cloned.1.call-start = ((), (), s32[]{:S(2)}) async-start(), calls=%async_computation.5 | async-start | bytes 2621440 | tf_op jit(solution)/shard_map/all_gather | solution.py:85
  9.3 196.9 %all-gather.22.cloned.1.call-start = ((), (), s32[]{:S(2)}) async-start(), calls=%async_computation.6 | async-start | bytes 2621440 | tf_op jit(solution)/shard_map/all_gather | solution.py:86
  9.9 242.3 %all-gather.26.cloned.1.call-start = ((), (), s32[]{:S(2)}) async-start(), calls=%async_computation.9 | async-start | bytes 2621440 | tf_op jit(solution)/shard_map/all_gather | solution.py:21
  10.0 2.6 copy-start.9
  12.6 4.4 %copy-start.12 = (f32[512]{0:T(512)S(1)}, f32[512]{0:T(512)}, u32[]{:S(2)}) copy-start(f32[512]{0:T(512)} %param.30) | copy-start | bytes 6148
  12.6 4.5 %copy-start.13 = (f32[1,768,256]{2,1,0:T(8,128)S(1)}, f32[1,768,256]{2,1,0:T(8,128)}, u32[]{:S(2)}) copy-start(f32[1,768,256]{2,1,0:T(8,128)} %param.31) | copy-start | bytes 2359300
  12.6 4.5 %copy-start.14 = (bf16[16,512]{1,0:T(8,128)(2,1)S(1)}, bf16[16,512]{1,0:T(8,128)(2,1)}, u32[]{:S(2)}) copy-start(bf16[16,512]{1,0:T(8,128)(2,1)} %param.29) | copy-start | bytes 49156
  41.7 48.1 %copy-start.7 = (bf16[768,256]{1,0:T(8,128)(2,1)}, bf16[768,256]{1,0:T(8,128)(2,1)S(1)}, u32[]{:S(2)}) copy-start(bf16[768,256]{1,0:T(8,128)(2,1)S(1)} %convolution_convert_fusion.1) | copy-start | bytes 1179652
  89.8 4.7 %copy-start.5 = (bf16[768,512]{1,0:T(8,128)(2,1)}, bf16[768,512]{1,0:T(8,128)(2,1)S(1)}, u32[]{:S(2)}) copy-start(bf16[768,512]{1,0:T(8,128)(2,1)S(1)} %convolution_convert_fusion) | copy-start | bytes 2359300
  118.8 0.8 copy-start.2
  119.7 9.8 %copy-start.11 = (f32[1024]{0:T(1024)S(1)}, f32[1024]{0:T(1024)}, u32[]{:S(2)}) copy-start(f32[1024]{0:T(1024)} %param.34) | copy-start | bytes 12292
  119.7 178.6 %all-gather.18.cloned.1.call-start = ((), (), s32[]{:S(2)}) async-start(), calls=%async_computation.4 | async-start | bytes 2621440 | tf_op jit(solution)/shard_map/all_gather | solution.py:178
  120.4 223.9 %all-gather.24.cloned.1.call-start = ((), (), s32[]{:S(2)}) async-start(), calls=%async_computation.7 | async-start | bytes 2621440 | tf_op jit(solution)/shard_map/all_gather | solution.py:179
  121.2 245.7 %reduce-scatter.2.cloned.1.call-start = ((), (), s32[]{:S(2)}) async-start(), calls=%async_computation.8 | async-start | bytes 9437184 | tf_op jit(solution)/shard_map/reduce_scatter | solution.py:184
  135.4 1.0 copy-start.8
  211.2 10.0 %collective-permute-start = (bf16[30,512]{1,0:T(8,128)(2,1)S(1)}, bf16[30,512]{1,0:T(8,128)(2,1)S(1)}, u32[]{:S(2)}, u32[]{:S(2)}) collective-permute-start(bf16[30,512]{1,0:T(8,128)(2,1)S(1)} %slice.257), channel_id=1, source_target_pairs={{0,8},{8,16},{16,24},{1,9},{9,17},{17,25},{2,10},{10,18},{18,26},{... | collective-permute-start | bytes 92168 | tf_op jit(solution)/shard_map/ppermute | solution.py:39
  252.2 4.9 %copy-start.4 = (f32[768,256]{1,0:T(8,128)S(1)}, f32[768,256]{1,0:T(8,128)}, u32[]{:S(2)}) copy-start(f32[768,256]{1,0:T(8,128)} %get-tuple-element.254) | copy-start | bytes 2359300
  257.1 2.8 copy-start.3
  257.1 2.8 copy-start.6
  259.9 1.1 copy-start.10
  352.4 17.7 %copy-start.1 = (bf16[2048,16]{0,1:T(8,128)(2,1)S(1)}, bf16[2048,16]{0,1:T(8,128)(2,1)}, u32[]{:S(2)}) copy-start(bf16[2048,16]{0,1:T(8,128)(2,1)} %param.28) | copy-start | bytes 196612
Sparse Core Ops, SparseCore 0:
  8.9 29.5 all-gather.13
  40.1 45.3 all-gather.15
  87.0 26.4 all-gather.11
  115.0 45.3 all-gather.19
  161.8 44.3 all-gather.21
  207.7 44.4 all-gather.25
  253.7 44.4 all-gather.17
  299.8 44.4 all-gather.23
  352.6 14.2 reduce-scatter.1
where the time goes:
time: 378 us; the launch traced here: 377 us
  waiting for transfers between devices  240 us (63%)
  matrix products  57.6 us (15%)
  other arithmetic  48.1 us (13%)
  between operations  13.6 us (4%)
  blocking collectives  11.5 us (3%)
  local copies, waits for them, and re-layouts  4.17 us (1%)
    all_gather x1, waiting for transfers between devices, on_device(): lax.all_gather(w_value, 'sp', axis=0, tiled=True)  43.8 us
    all_gather x1, waiting for transfers between devices, on_device(): lax.all_gather(w_conv_gate, 'sp', axis=0, tiled=True)  40.4 us
    all_gather x1, waiting for transfers between devices, on_device(): lax.all_gather(w_out_conv, 'sp', axis=1, tiled=True)  40 us
    all_gather x1, waiting for transfers between devices, on_device(): lax.all_gather(w_out_attn, 'sp', axis=1, tiled=True)  37 us
    all_gather x1, waiting for transfers between devices, on_device(): lax.all_gather(w_conv_value, 'sp', axis=0, tiled=True)  22.2 us
    dot_general x5, matrix products, on_device(): jnp.dot(normed, weight_piece, preferred_element_type=jnp.float32)  21.1 us
    all_gather x1, waiting for transfers between devices, entering(): everything = jax.tree.map(lambda part: lax.all_gather(part, axis), array)  20.1 us
    all_gather x1, waiting for transfers between devices, on_device(): lax.all_gather(w_key, 'sp', axis=0, tiled=True)  17.1 us
  transfers between devices with their start and end apart: 10, of which 8 were waited for; matrix products, arithmetic and copies ran while one was open for 26% of the time, Pallas kernels for 0%

commit v1 on v0

--- a/solution.py
+++ b/solution.py
@@ -41,6 +41,16 @@
 
 def rounded(array):
     return lax.optimization_barrier(array.astype(jnp.bfloat16)).astype(jnp.float32)
+
+
+def spread_gather(*weights):
+    turns = lax.axis_size("fs")
+    rows = weights[0].shape[0] // turns
+    start = lax.axis_index("fs") * rows
+    piece = jnp.concatenate(
+        [lax.dynamic_slice_in_dim(weight, start, rows, 0) for weight in weights], axis=1
+    )
+    return lax.all_gather(piece, ("sp", "fs"), axis=0, tiled=True)
 
 
 def chain_combine(earlier, later):
@@ -78,19 +88,16 @@
     value_cols = w_value.shape[1]
     conv_cols = w_conv_value.shape[1]
     heads_here = key_cols // DK
-    pieces = (
-        lax.all_gather(w_query, "sp", axis=0, tiled=True),
-        lax.all_gather(w_key, "sp", axis=0, tiled=True),
-        lax.all_gather(w_value, "sp", axis=0, tiled=True),
-        lax.all_gather(w_conv_value, "sp", axis=0, tiled=True),
-        lax.all_gather(w_conv_gate, "sp", axis=0, tiled=True),
-    )
-    queries, keys_proj, values_proj, conv_value, conv_gate = tuple(
-        (
-            jnp.dot(normed, weight_piece, preferred_element_type=jnp.float32)
-            for weight_piece in pieces
-        )
-    )
+    qkv_weight = spread_gather(w_query, w_key, w_value)
+    conv_weight = spread_gather(w_conv_value, w_conv_gate)
+    out_weight = spread_gather(w_out_attn, w_out_conv)
+    qkv = jnp.dot(normed, qkv_weight, preferred_element_type=jnp.float32)
+    queries = qkv[:, :key_cols]
+    keys_proj = qkv[:, key_cols : 2 * key_cols]
+    values_proj = qkv[:, 2 * key_cols :]
+    both = jnp.dot(normed, conv_weight, preferred_element_type=jnp.float32)
+    conv_value = both[:, :conv_cols]
+    conv_gate = both[:, conv_cols:]
     low_rank = jnp.dot(normed, w_decay_low, preferred_element_type=jnp.float32).astype(jnp.bfloat16)
     high_cols = lax.dynamic_slice_in_dim(w_decay_high, position * key_cols, key_cols, 1)
     bias_here = lax.dynamic_slice_in_dim(gate_bias, position * key_cols, key_cols, 0)
@@ -174,14 +181,21 @@
     variance = square_sum / CW - mean * mean
     gain_here = lax.dynamic_slice_in_dim(channel_gain, position * conv_cols, conv_cols, 0)
     conv_out = jax.nn.silu(centered * lax.rsqrt(variance + LN_EPS) * gain_here).astype(jnp.bfloat16)
-    pieces = (
-        lax.all_gather(w_out_attn, "sp", axis=1, tiled=True),
-        lax.all_gather(w_out_conv, "sp", axis=1, tiled=True),
-    )
-    columns = jnp.dot(attn_out, pieces[0], preferred_element_type=jnp.float32) + jnp.dot(
-        conv_out, pieces[1], preferred_element_type=jnp.float32
-    )
-    mixed = lax.psum_scatter(columns, "tp", scatter_dimension=0, tiled=True)
+    parts = lax.axis_size("sp")
+    width = w_out_attn.shape[1]
+    out_weight = out_weight.reshape(parts, value_cols, 2 * width)
+    columns = jnp.concatenate(
+        [
+            jnp.dot(attn_out, out_weight[z, :, :width], preferred_element_type=jnp.float32)
+            + jnp.dot(conv_out, out_weight[z, :, width:], preferred_element_type=jnp.float32)
+            for z in range(parts)
+        ],
+        axis=1,
+    )
+    half = length_here // 2
+    kept = lax.dynamic_slice_in_dim(columns, position * half, half, 0)
+    given = lax.dynamic_slice_in_dim(columns, (1 - position) * half, half, 0).astype(jnp.bfloat16)
+    mixed = kept + lax.ppermute(given, "tp", [(0, 1), (1, 0)]).astype(jnp.float32)
     return mixed.astype(jnp.bfloat16)[None]
 
 

time: 378 us -> 317 us (0.84)
  waiting for transfers between devices: 240 us -> 176 us
  matrix products: 57.6 us -> 42.5 us
  local copies, waits for them, and re-layouts: 4.17 us -> 17.3 us
  starting transfers between devices: 1.78 us -> 6.26 us
    all_gather x7 -> x3, waiting for transfers between devices: 200 us -> 159 us  [spread_gather(): return lax.all_gather(piece, ('sp', 'fs'), axis=0, tiled=True)]
    reduce_scatter x1 -> x0, waiting for transfers between devices: 14.4 us -> none  [on_device(): mixed = lax.psum_scatter(columns, 'tp', scatter_dimension=0, tiled=True)]
    dot_general x7 -> x10, matrix products: 35.3 us -> 21.5 us  [the longest x1 6.6 us: on_device(): qkv = jnp.dot(normed, qkv_weight, preferred_element_type=jnp.float32)]
    all_gather x1, waiting for transfers between devices: 20.1 us -> 13.7 us  [entering(): everything = jax.tree.map(lambda part: lax.all_gather(part, axis), array)]
    unnamed x30 -> x100, local copies, waits for them, and re-layouts: 0.9 us -> 5.81 us
    unnamed x9 -> x4, waiting for transfers between devices: 4.57 us -> 0.07 us
    convert_element_type x1, other arithmetic: 4.4 us -> 0.44 us  [on_device(): glu = (conv_value * jax.nn.sigmoid(conv_gate)).astype(jnp.bfloat16)]
  transfers between devices with their start and end apart: 10 -> 6, of which waited for: 8 -> 5; matrix products, arithmetic and copies ran while one was open for 26% -> 27% of each run, Pallas kernels for 0% -> 0%
where the time goes in v1:
time: 317 us; the launch traced here: 316 us
  waiting for transfers between devices  176 us (56%)
  other arithmetic  46.8 us (15%)
  matrix products  42.5 us (13%)
  local copies, waits for them, and re-layouts  17.3 us (5%)
  between operations  13.9 us (4%)
  blocking collectives  12.7 us (4%)
  starting transfers between devices  6.26 us (2%)
    all_gather x3, waiting for transfers between devices, spread_gather(): return lax.all_gather(piece, ('sp', 'fs'), axis=0, tiled=True)  159 us
    add x12, other arithmetic, carry_step(): decay_now[..., None] * recurrent_state + update_now  14 us
    all_gather x1, waiting for transfers between devices, entering(): everything = jax.tree.map(lambda part: lax.all_gather(part, axis), array)  13.7 us
    dynamic_update_slice x12, other arithmetic, on_device(): lax.scan(carry_step, jnp.zeros((heads_here, DK, DV), jnp.float32), (block...  10.2 us
    dot_general x1, matrix products, on_device(): jnp.einsum('hnik,nhkv->hniv', scaled_query, before, precision=UPPER_PRECI...  8.29 us
    all_gather x1, blocking collectives, entering(): everything = jax.tree.map(lambda part: lax.all_gather(part, axis), array)  8.25 us
    reduce_sum x1, other arithmetic, on_device(): jnp.sum(filtered, axis=1, keepdims=True)  7.37 us
    dot_general x1, matrix products, on_device(): qkv = jnp.dot(normed, qkv_weight, preferred_element_type=jnp.float32)  6.6 us
  transfers between devices with their start and end apart: 6, of which 5 were waited for; matrix products, arithmetic and copies ran while one was open for 27% of the time, Pallas kernels for 0%

profile of v1, /device:TPU:1, one launch (start us, length us, event | category | flops | bytes accessed | tf_op | source)
XLA Modules:
  0.0 315.7 jit_solution(17114797971922723320)
XLA Ops:
  6.5 1.0 copy-done
  9.3 1.0 constant_dynamic-slice_fusion.3
  11.2 2.6 fusion.1
  13.9 3.5 %fusion.47 = f32[768,256]{1,0:T(8,128)S(1)} fusion(f32[1,768,256]{2,1,0:T(8,128)S(1)} %copy-done.46, bf16[2048,16]{0,1:T(8,128)(2,1)S(1)} %copy-done.47, f32[256]{0:T(256)S(1)} %dynamic_slice.65, bf16[16,512]{1,0:T(8,128)(2,1)S(1)} %copy-done.48, s32[]{:T(128)S(6)} %select_n.75, bf16[1,768,2048]{2,1,0:T(8,128)(2,1)} %param.21, f32[2048]{0:T(1024)S(1)} %copy-done.49, ...), kind=kOutput, calls=%fused_computation.109 | convolution fusion | flops 65089536 | bytes 4805636 | tf_op jit(solution)/shard_map/dot_general | solution.py:106
  18.2 68.0 %all-gather.8.cloned.1.call-done = bf16[2048,1024]{1,0:T(8,128)(2,1)} async-done(((bf16[128,1024]{1,0:T(8,128)(2,1)}), bf16[2048,1024]{1,0:T(8,128)(2,1)}) %all-gather.8.cloned.1.call-update) | async-done | bytes 4194320 | tf_op jit(solution)/shard_map/all_gather | solution.py:53
  86.2 6.6 %convolution_convert_fusion = bf16[768,1024]{1,0:T(8,128)(2,1)S(1)} fusion(bf16[2048,1024]{1,0:T(8,128)(2,1)} %all-gather.8.cloned.1.call-done, bf16[1,768,2048]{2,1,0:T(8,128)(2,1)} %param.21, f32[2048]{0:T(1024)S(1)} %copy-done.49, f32[768]{0:T(1024)S(1)} %add_rsqrt_fusion.1), kind=kOutput, calls=%fused_computation.20 | convolution fusion | flops 3228303360 | bytes 8924160 | tf_op jit(solution)/shard_map/dot_general | solution.py:94
  93.6 4.7 %convolution_bitcast_fusion = f32[12,1,256,512]{3,2,1,0:T(8,128)} fusion(bf16[12,64,512]{2,1,0:T(8,128)(2,1)S(1)} %bitcast.171, bf16[12,64,256]{2,1,0:T(8,128)(2,1)S(1)} %bitcast.173, f32[1,12,64,256]{3,1,2,0:T(8,128)S(1)} %get-tuple-element.289, f32[12,256]{1,0:T(8,128)S(1)} %get-tuple-element.251), kind=kOutput, calls=%fused_computation.18 | convolution fusion | flops 1208549376 | bytes 8269824 | tf_op jit(solution)/shard_map/hnjk,hnjv->hnkv/dot_general | solution.py:129
  98.3 24.5 %while.32 = (s32[]{:T(128)}, f32[1,256,512]{2,1,0:T(8,128)S(1)}, f32[12,1,256,512]{3,2,1,0:T(8,128)}, f32[12,1,256]{2,0,1:T(8,128)S(1)}, f32[12,1,256,512]{3,2,1,0:T(8,128)}, /*index=5*/s32[]{:T(128)}, s32[]{:T(128)}) while((s32[]{:T(128)}, f32[1,256,512]{2,1,0:T(8,128)S(1)}, f32[12,1,256,512]{3,2,1,0:T(8,128)}, ...), condition=%wide.region_3.4_spmd.clone, body=%wide.region_2.3_spmd.clone.sunk | while | flops 524291 | bytes 2624620 | solution.py:141
  99.2 1.2 bitcast_add_fusion.3
  101.2 1.2 bitcast_add_fusion.3
  103.3 1.2 bitcast_add_fusion.3
  105.3 1.2 bitcast_add_fusion.3
  107.3 1.2 bitcast_add_fusion.3
  109.4 1.2 bitcast_add_fusion.3
  111.4 1.2 bitcast_add_fusion.3
  113.4 1.2 bitcast_add_fusion.3
  115.4 1.3 bitcast_add_fusion.3
  117.6 1.2 bitcast_add_fusion.3
  119.6 1.2 bitcast_add_fusion.3
  121.7 1.2 bitcast_add_fusion.3
  123.7 1.0 constant_dynamic-slice_fusion.5
  125.5 1.3 copy.55
  127.5 8.2 %all-gather.2 = f32[4,1,256]{2,1,0:T(1,128)S(1)} all-gather(f32[1,1,256]{2,1,0:T(1,128)S(1)} %bitcast.220), channel_id=2, replica_groups=mesh['sp'=4,'fs'=4,'tp'=2] {'sp'}, dimensions={0}, use_global_device_ids=true | all-gather | bytes 5120 | tf_op jit(solution)/shard_map/all_gather | solution.py:21
  135.8 1.9 fusion.78
  138.3 1.9 constant_dynamic-slice_fusion.2
  140.2 22.9 %all-gather.12.cloned.1.call-done = bf16[2048,1024]{1,0:T(8,128)(2,1)} async-done(((bf16[128,1024]{1,0:T(8,128)(2,1)}), bf16[2048,1024]{1,0:T(8,128)(2,1)}) %all-gather.12.cloned.1.call-update) | async-done | bytes 4194320 | tf_op jit(solution)/shard_map/all_gather | solution.py:53
  163.2 6.2 %fusion.70 = f32[768,1024]{1,0:T(8,128)S(1)} fusion(bf16[2048,1024]{1,0:T(8,128)(2,1)} %all-gather.12.cloned.1.call-done, bf16[1,768,2048]{2,1,0:T(8,128)(2,1)} %param.21, f32[2048]{0:T(1024)S(1)} %copy-done.49, f32[768]{0:T(1024)S(1)} %add_rsqrt_fusion.1), kind=kOutput, calls=%fused_computation.162 | convolution fusion | flops 3227516928 | bytes 10497024 | tf_op jit(solution)/shard_map/dot_general | solution.py:98
  169.9 3.8 %collective-permute-start = (bf16[30,512]{1,0:T(8,128)(2,1)S(1)}, bf16[30,512]{1,0:T(8,128)(2,1)S(1)}, u32[]{:S(2)}, u32[]{:S(2)}) collective-permute-start(bf16[30,512]{1,0:T(8,128)(2,1)S(1)} %slice.318), channel_id=1, source_target_pairs={{0,8},{8,16},{16,24},{1,9},{9,17},{17,25},{2,10},{10,18},{18,26},{... | collective-permute-start | bytes 92168 | tf_op jit(solution)/shard_map/ppermute | solution.py:39
  173.8 8.3 %fusion.4 = f32[12,64,512]{2,1,0:T(8,128)} fusion(f32[12,1,256,512]{3,2,1,0:T(8,128)} %get-tuple-element.143, f32[12,64,256]{2,1,0:T(8,128)S(1)} %bitcast.169, f32[1,12,64,256]{3,1,2,0:T(8,128)S(1)} %get-tuple-element.289), kind=kOutput, calls=%fused_computation.14 | convolution fusion | flops 1208156160 | bytes 9437184 | tf_op jit(solution)/shard_map/hnik,nhkv->hniv/dot_general | solution.py:146
  182.1 1.8 convolution_multiply_fusion
  184.9 7.4 %fusion.75 = (f32[768]{0:T(1024)S(1)}, f32[768]{0:T(1024)S(1)}, f32[768,512]{1,0:T(8,128)}) fusion(f32[798,512]{1,0:T(8,128)S(1)} %maximum_convert_fusion, f32[512]{0:T(512)S(1)} %bitcast.201, f32[512]{0:T(512)S(1)} %bitcast.203, f32[512]{0:T(512)S(1)} %bitcast.204, f32[512]{0:T(512)S(1)} %bitcast.205, f32[512]{0:T(512)S(1)} %bitcast.206, ...), kind=kLoop, calls=%fused_computation.163 | loop fusion | flops 25164288 | bytes 50401280 | tf_op jit(solution)/shard_map/reduce_sum | solution.py:174
  192.3 4.5 %all-reduce = (f32[768,1]{0,1:T(1,128)S(1)}, f32[768,1]{0,1:T(1,128)S(1)}) all-reduce(f32[768,1]{0,1:T(1,128)S(1)} %broadcast_in_dim.39, f32[768,1]{0,1:T(1,128)S(1)} %broadcast_in_dim.40), channel_id=1, replica_groups=mesh['sp'=4,'fs'=4,'tp'=2] {'tp'}, use_global_device_ids=true, to_apply=%region_10.11 | all-reduce | flops 1536 | bytes 12288 | tf_op jit(solution)/shard_map/psum | solution.py:172
  196.8 13.7 %all-gather.14.cloned.1.call-done = f32[4,256,512]{2,1,0:T(8,128)} async-done(((f32[1,256,512]{2,1,0:T(8,128)}), f32[4,256,512]{2,1,0:T(8,128)}) %all-gather.14.cloned.1.call-update) | async-done | bytes 2097168 | tf_op jit(solution)/shard_map/all_gather | solution.py:21
  210.5 4.9 %while.33 = (s32[]{:T(128)}, f32[1,256]{1,0:T(1,128)S(1)}, f32[1,256,512]{2,1,0:T(8,128)S(1)}, s32[]{:T(128)}, f32[4,1,256]{2,1,0:T(1,128)S(1)}, /*index=5*/f32[4,1,256,512]{3,2,1,0:T(8,128)}, s32[]{:T(128)}, s32[]{:T(128)}) while((s32[]{:T(128)}, f32[1,256]{1,0:T(1,128)S(1)}, f32[1,256,512]{2,1,0:T(8,128)S(1)}, s32[]{:T(128)}, ...), condition=%wide.region_7.8_spmd.clone, body=%wide.region_6.7_spmd.clone.sunk | while | flops 525060 | bytes 1578107 | solution.py:33
  210.5 1.2 fusion.92
  211.8 1.2 fusion.92
  213.0 1.2 fusion.92
  214.2 1.2 fusion.92
  215.4 1.6 fusion.57
  217.0 1.1 multiply_reduce_fusion.1
  218.3 68.0 %all-gather.10.cloned.1.call-done = bf16[2048,1024]{1,0:T(8,128)(2,1)} async-done(((bf16[128,1024]{1,0:T(8,128)(2,1)}), bf16[2048,1024]{1,0:T(8,128)(2,1)}) %all-gather.10.cloned.1.call-update) | async-done | bytes 4194320 | tf_op jit(solution)/shard_map/all_gather | solution.py:53
  286.4 1.8 fusion.53
  288.2 1.7 fusion.54
  296.4 2.7 copy-done.3
  299.2 2.4 collective-permute-start.1
  301.6 3.2 %collective-permute-done.1 = bf16[384,2048]{0,1:T(8,128)(2,1)} collective-permute-done((bf16[384,2048]{0,1:T(8,128)(2,1)S(1)}, bf16[384,2048]{0,1:T(8,128)(2,1)}, u32[]{:S(2)}, u32[]{:S(2)}) %collective-permute-start.1) | collective-permute-done | bytes 1572896 | tf_op jit(solution)/shard_map/ppermute | solution.py:198
  304.8 2.8 fusion.6
  307.5 1.6 copy.57
  (172 shorter events, 25.6 us)
Async XLA Ops:
  6.5 1.0 copy-start
  6.5 79.6 %all-gather.8.cloned.1.call-start = ((), (), s32[]{:S(2)}) async-start(), calls=%async_computation | async-start | bytes 4456448 | tf_op jit(solution)/shard_map/all_gather | solution.py:53
  9.2 153.9 %all-gather.12.cloned.1.call-start = ((), (), s32[]{:S(2)}) async-start(), calls=%async_computation.2 | async-start | bytes 4456448 | tf_op jit(solution)/shard_map/all_gather | solution.py:53
  11.0 199.4 %all-gather.14.cloned.1.call-start = ((), (), s32[]{:S(2)}) async-start(), calls=%async_computation.3 | async-start | bytes 2621440 | tf_op jit(solution)/shard_map/all_gather | solution.py:21
  11.1 2.7 copy-start.45
  11.1 2.8 copy-start.46
  11.1 2.8 copy-start.47
  11.2 2.8 copy-start.48
  11.2 2.8 copy-start.49
  93.6 4.7 %copy-start.5 = (bf16[768,256]{1,0:T(8,128)(2,1)}, bf16[768,256]{1,0:T(8,128)(2,1)S(1)}, u32[]{:S(2)}) copy-start(bf16[768,256]{1,0:T(8,128)(2,1)S(1)} %get-tuple-element.249) | copy-start | bytes 1179652
  122.9 0.8 copy-start.2
  123.7 3.2 %copy-start.44 = (f32[1024]{0:T(1024)S(1)}, f32[1024]{0:T(1024)}, u32[]{:S(2)}) copy-start(f32[1024]{0:T(1024)} %param.34) | copy-start | bytes 12292
  123.7 162.7 %all-gather.10.cloned.1.call-start = ((), (), s32[]{:S(2)}) async-start(), calls=%async_computation.1 | async-start | bytes 4456448 | tf_op jit(solution)/shard_map/all_gather | solution.py:53
  169.4 4.3 %copy-start.7 = (f32[1,12,64,256]{3,2,1,0:T(8,128)S(1)}, f32[1,12,64,256]{3,2,1,0:T(8,128)}, u32[]{:S(2)}) copy-start(f32[1,12,64,256]{3,2,1,0:T(8,128)} %copy.55) | copy-start | bytes 2359300
  169.4 4.3 %copy-start.9 = (bf16[768,256]{1,0:T(8,128)(2,1)S(1)}, bf16[768,256]{1,0:T(8,128)(2,1)}, u32[]{:S(2)}) copy-start(bf16[768,256]{1,0:T(8,128)(2,1)} %get-tuple-element.250) | copy-start | bytes 1179652
  169.9 14.4 %collective-permute-start = (bf16[30,512]{1,0:T(8,128)(2,1)S(1)}, bf16[30,512]{1,0:T(8,128)(2,1)S(1)}, u32[]{:S(2)}, u32[]{:S(2)}) collective-permute-start(bf16[30,512]{1,0:T(8,128)(2,1)S(1)} %slice.318), channel_id=1, source_target_pairs={{0,8},{8,16},{16,24},{1,9},{9,17},{17,25},{2,10},{10,18},{18,26},{... | collective-permute-start | bytes 92168 | tf_op jit(solution)/shard_map/ppermute | solution.py:39
  173.8 8.3 %copy-start.6 = (bf16[768,256]{1,0:T(8,128)(2,1)S(1)}, bf16[768,256]{1,0:T(8,128)(2,1)}, u32[]{:S(2)}) copy-start(bf16[768,256]{1,0:T(8,128)(2,1)} %copy-done.5) | copy-start | bytes 1179652
  173.8 8.3 %copy-start.12 = (f32[64,64]{1,0:T(8,128)S(1)}, f32[64,64]{1,0:T(8,128)}, u32[]{:S(2)}) copy-start(f32[64,64]{1,0:T(8,128)} %fusion.67) | copy-start | bytes 49156
  183.9 0.7 copy-start.13
  184.0 0.7 copy-start.14
  184.0 0.7 copy-start.15
  184.0 0.7 copy-start.17
  184.0 0.7 copy-start.18
  184.0 0.7 copy-start.19
  184.0 0.7 copy-start.20
  184.0 0.7 copy-start.21
  184.0 0.7 copy-start.22
  184.0 0.7 copy-start.23
  184.1 0.7 copy-start.24
  184.1 0.7 copy-start.25
  184.1 0.7 copy-start.29
  184.1 0.7 copy-start.30
  184.1 0.7 copy-start.31
  184.1 0.7 copy-start.33
  184.2 0.7 copy-start.34
  184.2 0.7 copy-start.37
  184.2 0.7 copy-start.38
  184.2 0.7 copy-start.40
  184.2 0.7 copy-start.41
  210.5 4.9 %copy-start.11 = (f32[1,1,256,512]{3,2,1,0:T(8,128)S(1)}, f32[1,1,256,512]{3,2,1,0:T(8,128)}, u32[]{:S(2)}) copy-start(f32[1,1,256,512]{3,2,1,0:T(8,128)} %param.37) | copy-start | bytes 1572868
  215.4 1.6 copy-start.4
  217.0 1.1 copy-start.43
  286.3 3.5 %copy-start.10 = (bf16[2048,1024]{1,0:T(8,128)(2,1)S(1)}, bf16[2048,1024]{1,0:T(8,128)(2,1)}, u32[]{:S(2)}) copy-start(bf16[2048,1024]{1,0:T(8,128)(2,1)} %all-gather.10.cloned.1.call-done) | copy-start | bytes 12582916
  290.5 1.4 copy-start.8
  290.5 1.4 copy-start.42
  296.4 2.7 copy-start.3
  299.2 5.5 %collective-permute-start.1 = (bf16[384,2048]{0,1:T(8,128)(2,1)S(1)}, bf16[384,2048]{0,1:T(8,128)(2,1)}, u32[]{:S(2)}, u32[]{:S(2)}) collective-permute-start(bf16[384,2048]{0,1:T(8,128)(2,1)S(1)} %dynamic-slice_convert_fusion), channel_id=1, source_target_pairs={{0,1},{1,0},{2,3},{3,2},{4,5},{5,4},{6,7},{7,6},{8,9},{9,8},{10,11... | collective-permute-start | bytes 4718600 | tf_op jit(solution)/shard_map/ppermute | solution.py:198
  304.8 4.4 %copy-start.1 = (bf16[512,512]{1,0:T(8,128)(2,1)S(1)}, bf16[512,512]{1,0:T(8,128)(2,1)}, u32[]{:S(2)}) copy-start(bf16[512,512]{1,0:T(8,128)(2,1)} %param.25) | copy-start | bytes 1572868
  (8 other events, 5.3 us)
Sparse Core Ops, SparseCore 0:
  10.1 76.0 all-gather.7
  88.9 74.1 all-gather.11
  164.7 45.7 all-gather.13
  213.1 73.1 all-gather.9
